TPU v7x, 128 devices: a whole 4x4x4 slice. The times are simulated.
128 devices in a mesh: sp: 32 (over z, y, core), tp: 4 (over x).
Axes of the slice: x: 4, y: 4, z: 4, core: 2. Of those that a mesh axis runs over, the one named last changes fastest.
Arguments:
- residual_entry_input: bfloat16 [32768, 2048], P(('sp', 'tp')), may hold values from -6 to 6
- query_matrix_rows: bfloat16 [32768, 1024], P('sp', 'tp'), may hold values from -6 to 6
- key_matrix_rows: bfloat16 [32768, 1024], P('sp', 'tp'), may hold values from -6 to 6
- value_matrix_rows: bfloat16 [32768, 2048], P('sp', 'tp'), may hold values from -6 to 6
- output_gate_logits: bfloat16 [32768, 2048], P('sp', 'tp'), may hold values from -6 to 6
- input_gate_logits: float32 [32768, 8], P('sp', 'tp'), may hold values from -6 to 6
- forget_gate_logits: float32 [32768, 8], P('sp', 'tp'), may hold values from -8 to 31
- forget_decay_offset: float32 [32768, 8], P('sp', 'tp'), may hold values from -0.7 to 0
- head_norm_gain: float32 [8, 256], P('tp'), may hold values from 0.1 to 1.9
- cell_output_weight: bfloat16 [2048, 2048], P('tp'), may hold values from -0.125 to 0.125
- feedforward_norm_gain: float32 [2048], replicated, may hold values from 0.1 to 1.9
- gate_up_weight: bfloat16 [2048, 5632], P('sp', 'tp'), may hold values from -0.125 to 0.125
- value_up_weight: bfloat16 [2048, 5632], P('sp', 'tp'), may hold values from -0.125 to 0.125
- gate_filter_taps: float32 [3, 5632], P(None, 'tp'), may hold values from -3 to 3
- value_filter_taps: float32 [3, 5632], P(None, 'tp'), may hold values from -3 to 3
- down_projection_weight: bfloat16 [5632, 2048], P('tp', 'sp'), may hold values from -0.078125 to 0.078125
Outputs:
- result: bfloat16 [32768, 2048], P(('sp', 'tp'))
All inputs are finite; a program needn't handle non-finite values.
Results may differ from a plain program's by a relative error of at most 0.025.
Values may be sent and summed in bfloat16 or wider, within the bound.
A program may use at most 128 MiB of HBM per device.

v0:
```python
import jax
import jax.numpy as jnp
from jax import lax
from jax.sharding import Mesh
from jax.sharding import PartitionSpec as P

BLOCK = 128
SP = ("sp_0", "sp_1", "sp_2")
SP_TP = ("sp_0", "sp_1", "sp_2", "tp")
eps = 1e-06
neg_large = -1e30


def neutral_like(x, identity):
    return jax.tree.map(
        lambda part, zero: jnp.zeros_like(part) + jnp.asarray(zero, part.dtype), x, identity
    )


def gathered_once(x, axis):
    leaves = jax.tree.leaves(x)
    sequence = sorted(range(len(leaves)), key=lambda k: -leaves[k].size)
    width = (1, *leaves[sequence[0]].shape)[-1]
    lines = [
        jnp.pad(leaves[k].reshape(-1), (0, -leaves[k].size % width)).reshape(-1, width)
        for k in sequence
    ]
    both, at, found = (lax.all_gather(jnp.concatenate(lines), axis), 0, {})
    for k, line in zip(sequence, lines):
        slab = both[:, at : at + len(line)].reshape(len(both), -1)
        found[k] = slab[:, : leaves[k].size].reshape(-1, *leaves[k].shape)
        at += len(line)
    numbers = iter(range(len(leaves)))
    return jax.tree.map(lambda _: found[next(numbers)], x)


def entering(x, axes, combine, identity):
    before = start = neutral_like(x, identity)
    running = x
    for axis in reversed(axes):
        count, position = (lax.axis_size(axis), lax.axis_index(axis))
        pieces = gathered_once(
            jax.tree.map(
                lambda part, kind: part.astype(kind),
                running,
                (jnp.bfloat16, jnp.bfloat16, jnp.bfloat16, jnp.bfloat16),
            ),
            axis,
        )
        inside, running = (start, start)
        for k in range(count):
            passed = k < position
            running = combine(
                running, jax.tree.map(lambda part, own: part[k].astype(own.dtype), pieces, x)
            )
            inside = jax.tree.map(lambda new, old: jnp.where(passed, new, old), running, inside)
        before = combine(inside, before)
    return before


def shifted(x, axis, by):
    count = lax.axis_size(axis)
    pairs = [(i, i + by) for i in range(count) if 0 <= i + by < count]
    return lax.ppermute(x, axis, pairs)


def side_by_side(arrays, axis, dim, along):
    both = jnp.concatenate(arrays, axis=along)
    result, at, finished = (lax.all_gather(both, axis, axis=dim, tiled=True), 0, [])
    for a in arrays:
        finished.append(lax.slice_in_dim(result, at, at + a.shape[along], axis=along))
        at += a.shape[along]
    return tuple(finished)


def laid_out(tiles, dim):
    shape = list(tiles.shape[1:])
    shape[dim] *= tiles.shape[0]
    return jnp.moveaxis(tiles, 0, dim).reshape(shape)


def all_blocks(x, axes, sequence):
    tiles = x
    for k in sequence:
        tiles = lax.all_gather(tiles, axes[k])
    done = sequence[::-1]
    back = [done.index(k) for k in range(len(axes))]
    tiles = tiles.transpose(*back, *range(len(axes), tiles.ndim))
    return tiles.reshape(-1, *x.shape)


def gather_axes(x, axes, sequence, dim):
    return laid_out(all_blocks(x, axes, sequence), dim)


def gate_log_values(input_gate_logits, forget_gate_logits, forget_decay_offset):
    input_log_value = 15.0 * jnp.tanh(input_gate_logits / 15.0)
    forget_log_sigmoid = (
        jax.nn.log_sigmoid(15.0 * jnp.tanh(forget_gate_logits / 15.0)) + forget_decay_offset
    )
    return (input_log_value, forget_log_sigmoid)


def combine_states(earlier, later):
    total_one, memory_one, normer_one, running_one = earlier
    total_two, memory_two, normer_two, running_two = later
    joined = jnp.maximum(total_two + running_one, running_two)
    weight_one = jnp.exp(total_two + running_one - joined)
    weight_two = jnp.exp(running_two - joined)
    memory = weight_one[:, None, None] * memory_one + weight_two[:, None, None] * memory_two
    normer = weight_one[:, None] * normer_one + weight_two[:, None] * normer_two
    return (total_one + total_two, memory, normer, joined)


def local_step(state_carry, inputs):
    memory, normer, running = state_carry
    query_block, key_block, value_block, input_block, forget_block = inputs
    length = query_block.shape[0]
    highest = lax.Precision.DEFAULT
    query_scale = query_block.shape[2] ** (-0.5)
    causal = jnp.tril(jnp.ones((length, length), dtype=bool))[:, :, None]
    cumulative = jnp.cumsum(forget_block, axis=0)
    logits = cumulative[:, None, :] - cumulative[None, :, :] + input_block[None, :, :]
    logits = jnp.where(causal, logits, -jnp.inf)
    carried = cumulative + running[None, :]
    stable = jnp.maximum(carried, jnp.max(logits, axis=1))
    carry_weight = jnp.exp(carried - stable)
    raw = (
        jnp.einsum("thd,shd->tsh", query_block, key_block, preferred_element_type=jnp.float32)
        * query_scale
    )
    scores = raw * jnp.exp(logits - stable[:, None, :])
    scaled_query = query_block.astype(jnp.float32) * query_scale
    numerator = carry_weight[:, :, None] * jnp.einsum(
        "hvd,thd->thv", memory, scaled_query, precision=highest
    )
    numerator = numerator + jnp.einsum(
        "tsh,shv->thv", scores.astype(jnp.bfloat16), value_block, preferred_element_type=jnp.float32
    )
    denominator = carry_weight * jnp.einsum(
        "hd,thd->th", normer, scaled_query, precision=highest
    ) + jnp.sum(scores, axis=1)
    last_sum = cumulative[-1]
    weights_log = last_sum[None, :] - cumulative + input_block
    new_running = jnp.maximum(last_sum + running, jnp.max(weights_log, axis=0))
    decay_factor = jnp.exp(last_sum + running - new_running)
    weighted = (
        key_block.astype(jnp.float32) * jnp.exp(weights_log - new_running[None, :])[:, :, None]
    )
    memory = decay_factor[:, None, None] * memory + jnp.einsum(
        "shv,shd->hvd",
        value_block,
        weighted.astype(jnp.bfloat16),
        preferred_element_type=jnp.float32,
    )
    normer = decay_factor[:, None] * normer + jnp.sum(weighted, axis=0)
    return ((memory, normer, new_running), (numerator, denominator, stable))


def local(
    residual_entry_input,
    query_matrix_rows,
    key_matrix_rows,
    value_matrix_rows,
    output_gate_logits,
    input_gate_logits,
    forget_gate_logits,
    forget_decay_offset,
    head_norm_gain,
    cell_output_weight,
    feedforward_norm_gain,
    gate_up_weight,
    value_up_weight,
    gate_filter_taps,
    value_filter_taps,
    down_projection_weight,
):
    highest = lax.Precision.DEFAULT
    token_count = query_matrix_rows.shape[0]
    head_count = input_gate_logits.shape[1]
    key_width = query_matrix_rows.shape[1] // head_count
    value_width = value_matrix_rows.shape[1] // head_count
    query_scale = key_width ** (-0.5)
    queries_low = query_matrix_rows.reshape(token_count, head_count, key_width)
    keys_low = key_matrix_rows.reshape(token_count, head_count, key_width)
    values_low = value_matrix_rows.reshape(token_count, head_count, value_width)
    input_log_value, forget_log_sigmoid = gate_log_values(
        input_gate_logits, forget_gate_logits, forget_decay_offset
    )
    cumulative = jnp.cumsum(forget_log_sigmoid, axis=0)
    total_log = cumulative[-1]
    block_count = token_count // BLOCK

    def blocks(tensor):
        return tensor.reshape((block_count, BLOCK) + tensor.shape[1:])

    initial = (
        jnp.zeros((head_count, value_width, key_width), jnp.float32),
        jnp.zeros((head_count, key_width), jnp.float32),
        jnp.full((head_count,), neg_large, jnp.float32),
    )
    end_state, (numerator, denominator, stable) = lax.scan(
        local_step,
        initial,
        (
            blocks(queries_low),
            blocks(keys_low),
            blocks(values_low),
            blocks(input_log_value),
            blocks(forget_log_sigmoid),
        ),
    )
    end_memory, end_normer, end_running = end_state
    identity = (
        jnp.zeros((head_count,), jnp.float32),
        jnp.zeros((head_count, value_width, key_width), jnp.float32),
        jnp.zeros((head_count, key_width), jnp.float32),
        jnp.full((head_count,), neg_large, jnp.float32),
    )
    prefix = entering(
        (total_log, end_memory, end_normer, end_running), SP, combine_states, identity
    )
    numerator = numerator.reshape(token_count, head_count, value_width)
    denominator = denominator.reshape(token_count, head_count)
    stable = stable.reshape(token_count, head_count)
    _, prior_memory, prior_normer, prior_running = prefix
    scaled_query = queries_low.astype(jnp.float32) * query_scale
    prior_log = cumulative + prior_running[None, :]
    top_log = jnp.maximum(stable, prior_log)
    local_weight = jnp.exp(stable - top_log)
    prior_weight = jnp.exp(prior_log - top_log)
    numerator = local_weight[:, :, None] * numerator + prior_weight[:, :, None] * jnp.einsum(
        "hvd,thd->thv", prior_memory, scaled_query, precision=highest
    )
    denominator = local_weight * denominator + prior_weight * jnp.einsum(
        "hd,thd->th", prior_normer, scaled_query, precision=highest
    )
    memory_out = numerator / jnp.maximum(jnp.abs(denominator), jnp.exp(-top_log))[:, :, None]
    normed = (
        memory_out
        * lax.rsqrt(jnp.mean(memory_out * memory_out, axis=-1, keepdims=True) + eps)
        * head_norm_gain[None, :, :]
    )
    gated_rows = (
        normed.reshape(token_count, head_count * value_width)
        * jax.nn.sigmoid(output_gate_logits.astype(jnp.float32))
    ).astype(jnp.bfloat16)
    whole_out = lax.all_gather(cell_output_weight, "tp", axis=0, tiled=True)
    own_rows = lax.all_to_all(gated_rows, "tp", split_axis=0, concat_axis=1, tiled=True)
    mixed_rows = jnp.dot(own_rows, whole_out, preferred_element_type=jnp.float32)
    stream_wide = residual_entry_input.astype(jnp.float32) + mixed_rows
    stream = stream_wide.astype(jnp.bfloat16)
    stream_wide = lax.optimization_barrier(stream).astype(jnp.float32)
    normed_rows = (
        stream_wide
        * lax.rsqrt(jnp.mean(stream_wide * stream_wide, axis=-1, keepdims=True) + eps)
        * feedforward_norm_gain[None, :]
    ).astype(jnp.bfloat16)
    group_rows = lax.all_gather(normed_rows, "tp", axis=0, tiled=True)
    earlier_rows = shifted(group_rows[-2:], SP, 1)
    window = jnp.concatenate([earlier_rows, group_rows], axis=0)
    pieces = side_by_side((gate_up_weight, value_up_weight), SP, 0, 1)
    up_gate = jnp.dot(window, pieces[0], preferred_element_type=jnp.float32)
    up_value = jnp.dot(window, pieces[1], preferred_element_type=jnp.float32)
    conv_g = (
        gate_filter_taps[0][None, :] * up_gate[:-2]
        + gate_filter_taps[1][None, :] * up_gate[1:-1]
        + gate_filter_taps[2][None, :] * up_gate[2:]
    )
    conv_v = (
        value_filter_taps[0][None, :] * up_value[:-2]
        + value_filter_taps[1][None, :] * up_value[1:-1]
        + value_filter_taps[2][None, :] * up_value[2:]
    )
    hidden = (jax.nn.silu(conv_g) * conv_v).astype(jnp.bfloat16)
    whole_down = gather_axes(down_projection_weight, (("sp_0", "sp_1"), "sp_2"), (0, 1), 1)
    ffn_rows = lax.psum_scatter(
        jnp.dot(hidden, whole_down, preferred_element_type=jnp.float32).astype(jnp.bfloat16),
        "tp",
        scatter_dimension=0,
        tiled=True,
    ).astype(jnp.float32)
    return (stream_wide + ffn_rows).astype(jnp.bfloat16)


def solution(mesh):
    split = Mesh(mesh.devices.reshape(4, 4, 2, mesh.shape["tp"]), ("sp_0", "sp_1", "sp_2", "tp"))
    placed = (
        P(SP_TP, None),
        P(SP, "tp"),
        P(SP, "tp"),
        P(SP, "tp"),
        P(SP, "tp"),
        P(SP, "tp"),
        P(SP, "tp"),
        P(SP, "tp"),
        P("tp", None),
        P("tp", None),
        P(),
        P(SP, "tp"),
        P(SP, "tp"),
        P(None, "tp"),
        P(None, "tp"),
        P("tp", SP),
    )
    return jax.shard_map(
        local, mesh=split, in_specs=placed, out_specs=P(SP_TP, None), check_vma=False
    )
```

profile of v0, /device:TPU:1, one launch (start us, length us, event | category | flops | bytes accessed | tf_op | source)
XLA Modules:
  0.0 419.1 jit_solution(10256180526580571442)
XLA Ops:
  9.1 1.3 reshape.1706
  11.7 2.0 reshape.1708
  13.6 102.5 %while.21 = (s32[]{:T(128)}, f32[2,256,128]{2,1,0:T(8,128)S(1)}, f32[2,128]{1,0:T(2,128)S(1)}, f32[2]{0:T(128)S(1)}, f32[8,128,2,256]{1,0,3,2:T(8,128)}, /*index...) while((s32[]{:T(128)}, f32[2,256,128]{2,1,0:T(8,128)S(1)}, ...), condition=%wide.region_6.7_spmd.clone, body=%wide.region_0.6_spmd.clone.sunk | while | flops 59952648 | bytes 4685610 | solution.py:202
  17.8 8.3 %dynamic_update_slice.19 = f32[8,128,2,256]{1,0,3,2:T(8,128)} dynamic-update-slice(f32[8,128,2,256]{1,0,3,2:T(8,128)} %get-tuple-element.428, f32[1,128,2,256]{1,0,3,2:T(1,128)S(1)} %copy.336, s32[]{:T(128)} %get-tuple-element.424, s32[]{:T(128)} %constant.38.clone.1..sunk, s32[]{:T(128)} %constant.38.clone.1..sunk, s32[]{:T(128)} %constant.38.clone.1..sunk) | dynamic-update-slice | bytes 524292 | tf_op jit(solution)/shard_map/while/body/jit(dynamic_update_index_in_dim)/dynamic_update_slice | solution.py:202
  30.7 8.2 %dynamic_update_slice.19 = f32[8,128,2,256]{1,0,3,2:T(8,128)} dynamic-update-slice(f32[8,128,2,256]{1,0,3,2:T(8,128)} %get-tuple-element.428, f32[1,128,2,256]{1,0,3,2:T(1,128)S(1)} %copy.336, s32[]{:T(128)} %get-tuple-element.424, s32[]{:T(128)} %constant.38.clone.1..sunk, s32[]{:T(128)} %constant.38.clone.1..sunk, s32[]{:T(128)} %constant.38.clone.1..sunk) | dynamic-update-slice | bytes 524292 | tf_op jit(solution)/shard_map/while/body/jit(dynamic_update_index_in_dim)/dynamic_update_slice | solution.py:202
  43.5 8.2 %dynamic_update_slice.19 = f32[8,128,2,256]{1,0,3,2:T(8,128)} dynamic-update-slice(f32[8,128,2,256]{1,0,3,2:T(8,128)} %get-tuple-element.428, f32[1,128,2,256]{1,0,3,2:T(1,128)S(1)} %copy.336, s32[]{:T(128)} %get-tuple-element.424, s32[]{:T(128)} %constant.38.clone.1..sunk, s32[]{:T(128)} %constant.38.clone.1..sunk, s32[]{:T(128)} %constant.38.clone.1..sunk) | dynamic-update-slice | bytes 524292 | tf_op jit(solution)/shard_map/while/body/jit(dynamic_update_index_in_dim)/dynamic_update_slice | solution.py:202
  56.3 8.2 %dynamic_update_slice.19 = f32[8,128,2,256]{1,0,3,2:T(8,128)} dynamic-update-slice(f32[8,128,2,256]{1,0,3,2:T(8,128)} %get-tuple-element.428, f32[1,128,2,256]{1,0,3,2:T(1,128)S(1)} %copy.336, s32[]{:T(128)} %get-tuple-element.424, s32[]{:T(128)} %constant.38.clone.1..sunk, s32[]{:T(128)} %constant.38.clone.1..sunk, s32[]{:T(128)} %constant.38.clone.1..sunk) | dynamic-update-slice | bytes 524292 | tf_op jit(solution)/shard_map/while/body/jit(dynamic_update_index_in_dim)/dynamic_update_slice | solution.py:202
  69.1 8.2 %dynamic_update_slice.19 = f32[8,128,2,256]{1,0,3,2:T(8,128)} dynamic-update-slice(f32[8,128,2,256]{1,0,3,2:T(8,128)} %get-tuple-element.428, f32[1,128,2,256]{1,0,3,2:T(1,128)S(1)} %copy.336, s32[]{:T(128)} %get-tuple-element.424, s32[]{:T(128)} %constant.38.clone.1..sunk, s32[]{:T(128)} %constant.38.clone.1..sunk, s32[]{:T(128)} %constant.38.clone.1..sunk) | dynamic-update-slice | bytes 524292 | tf_op jit(solution)/shard_map/while/body/jit(dynamic_update_index_in_dim)/dynamic_update_slice | solution.py:202
  81.9 8.2 %dynamic_update_slice.19 = f32[8,128,2,256]{1,0,3,2:T(8,128)} dynamic-update-slice(f32[8,128,2,256]{1,0,3,2:T(8,128)} %get-tuple-element.428, f32[1,128,2,256]{1,0,3,2:T(1,128)S(1)} %copy.336, s32[]{:T(128)} %get-tuple-element.424, s32[]{:T(128)} %constant.38.clone.1..sunk, s32[]{:T(128)} %constant.38.clone.1..sunk, s32[]{:T(128)} %constant.38.clone.1..sunk) | dynamic-update-slice | bytes 524292 | tf_op jit(solution)/shard_map/while/body/jit(dynamic_update_index_in_dim)/dynamic_update_slice | solution.py:202
  94.7 8.2 %dynamic_update_slice.19 = f32[8,128,2,256]{1,0,3,2:T(8,128)} dynamic-update-slice(f32[8,128,2,256]{1,0,3,2:T(8,128)} %get-tuple-element.428, f32[1,128,2,256]{1,0,3,2:T(1,128)S(1)} %copy.336, s32[]{:T(128)} %get-tuple-element.424, s32[]{:T(128)} %constant.38.clone.1..sunk, s32[]{:T(128)} %constant.38.clone.1..sunk, s32[]{:T(128)} %constant.38.clone.1..sunk) | dynamic-update-slice | bytes 524292 | tf_op jit(solution)/shard_map/while/body/jit(dynamic_update_index_in_dim)/dynamic_update_slice | solution.py:202
  107.5 8.2 %dynamic_update_slice.19 = f32[8,128,2,256]{1,0,3,2:T(8,128)} dynamic-update-slice(f32[8,128,2,256]{1,0,3,2:T(8,128)} %get-tuple-element.428, f32[1,128,2,256]{1,0,3,2:T(1,128)S(1)} %copy.336, s32[]{:T(128)} %get-tuple-element.424, s32[]{:T(128)} %constant.38.clone.1..sunk, s32[]{:T(128)} %constant.38.clone.1..sunk, s32[]{:T(128)} %constant.38.clone.1..sunk) | dynamic-update-slice | bytes 524292 | tf_op jit(solution)/shard_map/while/body/jit(dynamic_update_index_in_dim)/dynamic_update_slice | solution.py:202
  117.4 3.0 all-gather.5
  122.3 13.0 %all-gather.6 = bf16[4,516,128]{2,1,0:T(8,128)(2,1)S(1)} all-gather(bf16[1,516,128]{2,1,0:T(8,128)(2,1)S(1)} %maximum_bitcast_fusion.1), channel_id=3, replica_groups=mesh['sp_0'=4,'sp_1'=4,'sp_2'=2,'tp'=4] {'sp_1'}, dimensions={0}, use_global_device_ids=true | all-gather | bytes 660480 | tf_op jit(solution)/shard_map/all_gather | solution.py:28
  136.8 14.1 %all-gather.7 = bf16[4,516,128]{2,1,0:T(8,128)(2,1)S(1)} all-gather(bf16[1,516,128]{2,1,0:T(8,128)(2,1)S(1)} %maximum_bitcast_fusion.2), channel_id=4, replica_groups=mesh['sp_0'=4,'sp_1'=4,'sp_2'=2,'tp'=4] {'sp_0'}, dimensions={0}, use_global_device_ids=true | all-gather | bytes 660480 | tf_op jit(solution)/shard_map/all_gather | solution.py:28
  151.4 1.7 reshape.1638
  154.1 1.3 fusion.47
  157.2 1.9 copy.197
  159.2 2.5 multiply_convert_fusion
  161.7 14.4 %all_to_all.19 = bf16[4,256,512]{2,1,0:T(8,128)(2,1)S(1)} all-to-all(bf16[4,256,512]{2,1,0:T(8,128)(2,1)S(1)} %bitcast.610), channel_id=1, replica_groups=mesh['sp_0'=4,'sp_1'=4,'sp_2'=2,'tp'=4] {'tp'}, dimensions={0} | all-to-all | bytes 2097152 | tf_op jit(solution)/shard_map/all_to_all | solution.py:249
  176.6 5.7 %fusion.40 = bf16[256,2048]{1,0:T(8,128)(2,1)S(1)} fusion(bf16[256,2048]{0,1:T(8,128)(2,1)S(1)} %bitcast.606, bf16[2048,2048]{1,0:T(8,128)(2,1)} %all-gather.14.cloned.1.call-done, bf16[256,2048]{1,0:T(8,128)(2,1)S(1)} %copy-done), kind=kOutput, calls=%fused_computation.77 | convolution fusion | flops 2149056512 | bytes 11534336 | tf_op jit(solution)/shard_map/dot_general | solution.py:250
  182.7 1.3 fusion.43
  184.1 3.8 copy.246
  188.9 45.1 %all-gather.16.cloned.1.call-done = bf16[1024,2048]{1,0:T(8,128)(2,1)} async-done(((bf16[256,2048]{1,0:T(8,128)(2,1)}), bf16[1024,2048]{1,0:T(8,128)(2,1)}) %all-gather.16.cloned.1.call-update) | async-done | bytes 4194320 | tf_op jit(solution)/shard_map/all_gather | solution.py:259
  234.8 4.0 collective-permute-start
  238.9 16.3 %all-gather.22.cloned.1.call-done = bf16[32,1408,64]{1,0,2:T(8,128)(2,1)} async-done(((bf16[16,1408,64]{1,0,2:T(8,128)(2,1)}), bf16[32,1408,64]{1,0,2:T(8,128)(2,1)}) %all-gather.22.cloned.1.call-update) | async-done | bytes 5767184 | tf_op jit(solution)/shard_map/all_gather | solution.py:85
  255.2 7.0 %copy.200 = bf16[16,2,1408,64]{2,3,1,0:T(8,128)(2,1)} copy(bf16[16,2,1408,64]{2,0,1,3:T(8,128)(2,1)} %bitcast.607) | data formatting | bytes 11534336 | tf_op jit(solution)/shard_map/transpose | solution.py:88
  262.2 56.7 %all-gather.18.cloned.1.call-done = bf16[2048,2816]{1,0:T(8,128)(2,1)} async-done(((bf16[64,2816]{1,0:T(8,128)(2,1)}), bf16[2048,2816]{1,0:T(8,128)(2,1)}) %all-gather.18.cloned.1.call-update) | async-done | bytes 11534352 | tf_op jit(solution)/shard_map/all_gather | solution.py:69
  318.9 11.9 %fusion.37 = f32[1026,1408]{1,0:T(8,128)} fusion(bf16[2048,2816]{1,0:T(8,128)(2,1)} %all-gather.18.cloned.1.call-done, bf16[1024,2048]{1,0:T(8,128)(2,1)} %all-gather.16.cloned.1.call-done, bf16[2,2048]{1,0:T(2,128)(2,1)S(1)} %collective-permute-done), kind=kOutput, calls=%fused_computation.69 | convolution fusion | flops 5925519360 | bytes 15748096 | tf_op jit(solution)/shard_map/dot_general | solution.py:263
  330.9 8.7 %fusion.33 = f32[1026,1408]{1,0:T(8,128)} fusion(bf16[2048,2816]{1,0:T(8,128)(2,1)S(1)} %copy-done.13, bf16[1024,2048]{1,0:T(8,128)(2,1)S(1)} %copy-done.12, bf16[2,2048]{1,0:T(2,128)(2,1)S(1)} %collective-permute-done), kind=kOutput, calls=%fused_computation.62 | convolution fusion | flops 5925519360 | bytes 15748096 | tf_op jit(solution)/shard_map/dot_general | solution.py:264
  339.5 24.1 %convolution_convert_fusion = bf16[1024,2048]{1,0:T(8,128)(2,1)} fusion(bf16[1408,2048]{0,1:T(8,128)(2,1)} %bitcast.608, f32[1026,1408]{1,0:T(8,128)} %fusion.33, f32[1026,1408]{1,0:T(8,128)} %fusion.37, f32[1408]{0:T(1024)S(1)} %get-tuple-element.181, f32[1408]{0:T(1024)S(1)} %get-tuple-element.182, f32[1408]{0:T(1024)S(1)} %get-tuple-element.180, ...), kind=kOutput, calls=%fused_computation.72 | convolution fusion | flops 5930745856 | bytes 44598272 | tf_op jit(solution)/shard_map/dot_general | solution.py:278
  363.7 46.0 %reduce-scatter.2.cloned.1.call-done = bf16[256,2048]{1,0:T(8,128)(2,1)} async-done(((bf16[1024,2048]{1,0:T(8,128)(2,1)}), bf16[256,2048]{1,0:T(8,128)(2,1)}) %reduce-scatter.2.cloned.1.call-update) | async-done | bytes 1048592 | tf_op jit(solution)/shard_map/reduce_scatter | solution.py:277
  409.7 2.6 fusion.44
  (357 shorter events, 49.6 us)
Async XLA Ops:
  6.5 3.9 copy-start.10
  6.5 4.2 copy-start.1
  6.5 170.0 %all-gather.14.cloned.1.call-start = ((), (), s32[]{:S(2)}) async-start(), calls=%async_computation.2 | async-start | bytes 10485760 | tf_op jit(solution)/shard_map/all_gather | solution.py:248
  7.3 176.8 %all-gather.20.cloned.1.call-start = ((), (), s32[]{:S(2)}) async-start(), calls=%async_computation.6 | async-start | bytes 3063808 | tf_op jit(solution)/shard_map/all_gather | solution.py:85
  8.0 226.0 %all-gather.16.cloned.1.call-start = ((), (), s32[]{:S(2)}) async-start(), calls=%async_computation.3 | async-start | bytes 5242880 | tf_op jit(solution)/shard_map/all_gather | solution.py:259
  116.1 34.9 %copy-start.4 = (f32[8,128,2]{2,1,0:T(8,128)S(1)}, f32[8,128,2]{2,1,0:T(8,128)}, u32[]{:S(2)}) copy-start(f32[8,128,2]{2,1,0:T(8,128)} %get-tuple-element.72) | copy-start | bytes 24580
  116.1 35.1 %copy-start.3 = (f32[8,128,2]{2,1,0:T(8,128)S(1)}, f32[8,128,2]{2,1,0:T(8,128)}, u32[]{:S(2)}) copy-start(f32[8,128,2]{2,1,0:T(8,128)} %get-tuple-element.77) | copy-start | bytes 24580
  153.1 2.6 copy-start.2
  155.7 1.3 copy-start.11
  159.2 17.4 %copy-start = (bf16[256,2048]{1,0:T(8,128)(2,1)S(1)}, bf16[256,2048]{1,0:T(8,128)(2,1)}, u32[]{:S(2)}) copy-start(bf16[256,2048]{1,0:T(8,128)(2,1)} %param.18) | copy-start | bytes 3145732
  176.6 6.0 %copy-start.9 = (f32[2048]{0:T(1024)S(1)}, f32[2048]{0:T(1024)}, u32[]{:S(2)}) copy-start(f32[2048]{0:T(1024)} %param.28) | copy-start | bytes 24580
  184.0 71.2 %all-gather.22.cloned.1.call-start = ((), (), s32[]{:S(2)}) async-start(), calls=%async_computation.7 | async-start | bytes 8650752 | tf_op jit(solution)/shard_map/all_gather | solution.py:85
  184.0 4.0 copy-start.5
  184.0 4.0 copy-start.6
  184.1 54.8 %copy-start.7 = (f32[3,1408]{1,0:T(4,128)S(1)}, f32[3,1408]{1,0:T(4,128)}, u32[]{:S(2)}) copy-start(f32[3,1408]{1,0:T(4,128)} %param.32) | copy-start | bytes 50692
  184.1 54.8 %copy-start.8 = (f32[3,1408]{1,0:T(4,128)S(1)}, f32[3,1408]{1,0:T(4,128)}, u32[]{:S(2)}) copy-start(f32[3,1408]{1,0:T(4,128)} %param.31) | copy-start | bytes 50692
  187.9 131.0 %all-gather.18.cloned.1.call-start = ((), (), s32[]{:S(2)}) async-start(), calls=%async_computation.4 | async-start | bytes 11894784 | tf_op jit(solution)/shard_map/all_gather | solution.py:69
  188.8 220.8 %reduce-scatter.2.cloned.1.call-start = ((), (), s32[]{:S(2)}) async-start(), calls=%async_computation.5 | async-start | bytes 5242880 | tf_op jit(solution)/shard_map/reduce_scatter | solution.py:277
  234.8 27.4 %collective-permute-start = (bf16[2,2048]{1,0:T(2,128)(2,1)S(1)}, bf16[2,2048]{1,0:T(2,128)(2,1)S(1)}, u32[]{:S(2)}, u32[]{:S(2)}) collective-permute-start(bf16[2,2048]{1,0:T(2,128)(2,1)S(1)} %slice.352), channel_id=1, source_target_pairs={{0,4},{4,8},{8,12},{12,16},{16,20},{20,24},{24,28},{28,32},{32,36}... | collective-permute-start | bytes 24584 | tf_op jit(solution)/shard_map/ppermute | solution.py:64
  318.9 11.9 %copy-start.12 = (bf16[1024,2048]{1,0:T(8,128)(2,1)S(1)}, bf16[1024,2048]{1,0:T(8,128)(2,1)}, u32[]{:S(2)}) copy-start(bf16[1024,2048]{1,0:T(8,128)(2,1)} %all-gather.16.cloned.1.call-done) | copy-start | bytes 12582916
  318.9 11.9 %copy-start.13 = (bf16[2048,2816]{1,0:T(8,128)(2,1)S(1)}, bf16[2048,2816]{1,0:T(8,128)(2,1)}, u32[]{:S(2)}) copy-start(bf16[2048,2816]{1,0:T(8,128)(2,1)} %all-gather.18.cloned.1.call-done) | copy-start | bytes 34603012
Sparse Core Ops, SparseCore 0:
  9.0 86.0 all-gather.13
  97.3 51.0 all-gather.19
  184.1 49.8 all-gather.15
  235.5 19.6 all-gather.21
  257.3 61.5 all-gather.17
  363.8 45.7 reduce-scatter.1
where the time goes:
time: 421 us; the launch traced here: 419 us
  waiting for transfers between devices  166 us (39%)
  local copies, waits for them, and re-layouts  105 us (25%)
  matrix products  62 us (15%)
  blocking collectives  44.6 us (11%)
  other arithmetic  23.2 us (6%)
  between operations  14.1 us (3%)
  starting transfers between devices  4.22 us (1%)
    dynamic_update_slice x16, local copies, waits for them, and re-layouts, local(): lax.scan(local_step, initial, (blocks(queries_low), blocks(keys_low), blo...  66.9 us
    all_gather x1, waiting for transfers between devices, side_by_side(): lax.all_gather(both, axis, axis=dim, tiled=True)  56.7 us
    reduce_scatter x1, waiting for transfers between devices, local(): lax.psum_scatter(jnp.dot(hidden, whole_down, preferred_element_type=jnp.f...  46 us
    all_gather x1, waiting for transfers between devices, local(): group_rows = lax.all_gather(normed_rows, 'tp', axis=0, tiled=True)  45.1 us
    all_gather x3, blocking collectives, gathered_once(): both, at, found = (lax.all_gather(jnp.concatenate(lines), axis), 0, {})  30.2 us
    dot_general x1, matrix products, local(): jnp.dot(hidden, whole_down, preferred_element_type=jnp.float32)  24.1 us
    all_gather x2, waiting for transfers between devices, all_blocks(): tiles = lax.all_gather(tiles, axes[k])  16.3 us
    all_to_all x1, blocking collectives, local(): lax.all_to_all(gated_rows, 'tp', split_axis=0, concat_axis=1, tiled=True)  14.4 us
  transfers between devices with their start and end apart: 7, of which 4 were waited for; matrix products, arithmetic and copies ran while one was open for 34% of the time, Pallas kernels for 0%

commit v1 on v0

--- a/solution.py
+++ b/solution.py
@@ -256,7 +256,9 @@
         * lax.rsqrt(jnp.mean(stream_wide * stream_wide, axis=-1, keepdims=True) + eps)
         * feedforward_norm_gain[None, :]
     ).astype(jnp.bfloat16)
-    group_rows = lax.all_gather(normed_rows, "tp", axis=0, tiled=True)
+    group_rows = jnp.concatenate(
+        lax.all_to_all(jnp.stack([normed_rows] * lax.axis_size("tp")), "tp", 0, 0), axis=0
+    )
     earlier_rows = shifted(group_rows[-2:], SP, 1)
     window = jnp.concatenate([earlier_rows, group_rows], axis=0)
     pieces = side_by_side((gate_up_weight, value_up_weight), SP, 0, 1)

time: 421 us -> 398 us (0.945)
  waiting for transfers between devices: 166 us -> 97.6 us
  blocking collectives: 44.6 us -> 85.4 us
  starting transfers between devices: 4.22 us -> 10.2 us
    all_gather x1, waiting for transfers between devices: 56.7 us -> 0.01 us  [side_by_side(): lax.all_gather(both, axis, axis=dim, tiled=True)]
    all_gather x1 -> x0, waiting for transfers between devices: 45.1 us -> none  [local(): group_rows = lax.all_gather(normed_rows, 'tp', axis=0, tiled=True)]
    all_to_all x0 -> x1, blocking collectives: none -> 44.8 us  [local(): lax.all_to_all(jnp.stack([normed_rows] * lax.axis_size('tp')), 'tp', 0, 0)]
    all_gather x2, waiting for transfers between devices: 16.3 us -> 51.1 us  [all_blocks(): tiles = lax.all_gather(tiles, axes[k])]
    ppermute x1, starting transfers between devices: 4.02 us -> 10.1 us  [shifted(): return lax.ppermute(x, axis, pairs)]
  transfers between devices with their start and end apart: 7 -> 6, of which waited for: 4 -> 2; matrix products, arithmetic and copies ran while one was open for 34% -> 35% of each run, Pallas kernels for 0% -> 0%
where the time goes in v1:
time: 398 us; the launch traced here: 396 us
  local copies, waits for them, and re-layouts  106 us (27%)
  waiting for transfers between devices  97.6 us (25%)
  blocking collectives  85.4 us (21%)
  matrix products  60.7 us (15%)
  other arithmetic  21.6 us (5%)
  between operations  13.7 us (3%)
  starting transfers between devices  10.2 us (3%)
    dynamic_update_slice x16, local copies, waits for them, and re-layouts, local(): lax.scan(local_step, initial, (blocks(queries_low), blocks(keys_low), blo...  66.7 us
    all_gather x2, waiting for transfers between devices, all_blocks(): tiles = lax.all_gather(tiles, axes[k])  51.1 us
    reduce_scatter x1, waiting for transfers between devices, local(): lax.psum_scatter(jnp.dot(hidden, whole_down, preferred_element_type=jnp.f...  45 us
    all_to_all x1, blocking collectives, local(): lax.all_to_all(jnp.stack([normed_rows] * lax.axis_size('tp')), 'tp', 0, 0)  44.8 us
    all_gather x3, blocking collectives, gathered_once(): both, at, found = (lax.all_gather(jnp.concatenate(lines), axis), 0, {})  26.2 us
    dot_general x1, matrix products, local(): jnp.dot(hidden, whole_down, preferred_element_type=jnp.float32)  22.6 us
    all_to_all x1, blocking collectives, local(): lax.all_to_all(gated_rows, 'tp', split_axis=0, concat_axis=1, tiled=True)  14.4 us
    dot_general x1, matrix products, local(): up_gate = jnp.dot(window, pieces[0], preferred_element_type=jnp.float32)  11.9 us
  transfers between devices with their start and end apart: 6, of which 2 were waited for; matrix products, arithmetic and copies ran while one was open for 35% of the time, Pallas kernels for 0%

profile of v1, /device:TPU:1, one launch (start us, length us, event | category | flops | bytes accessed | tf_op | source)
XLA Modules:
  0.0 396.4 jit_solution(1212628433073211027)
XLA Ops:
  8.1 51.1 %all-gather.17.cloned.1.call-done = bf16[22528,64]{0,1:T(8,128)(2,1)} async-done(((bf16[1408,64]{0,1:T(8,128)(2,1)}), bf16[22528,64]{0,1:T(8,128)(2,1)}) %all-gather.17.cloned.1.call-update) | async-done | bytes 2883600 | tf_op jit(solution)/shard_map/all_gather | solution.py:85
  59.2 3.8 copy.246
  64.3 1.3 reshape.1712
  66.8 2.0 reshape.1714
  68.8 102.3 %while.21 = (s32[]{:T(128)}, f32[2,256,128]{2,1,0:T(8,128)S(1)}, f32[2,128]{1,0:T(2,128)S(1)}, f32[2]{0:T(128)S(1)}, f32[8,128,2,256]{1,0,3,2:T(8,128)}, /*index...) while((s32[]{:T(128)}, f32[2,256,128]{2,1,0:T(8,128)S(1)}, ...), condition=%wide.region_6.7_spmd.clone, body=%wide.region_0.6_spmd.clone.sunk | while | flops 59952648 | bytes 4685610 | solution.py:202
  73.0 8.2 %dynamic_update_slice.19 = f32[8,128,2,256]{1,0,3,2:T(8,128)} dynamic-update-slice(f32[8,128,2,256]{1,0,3,2:T(8,128)} %get-tuple-element.428, f32[1,128,2,256]{1,0,3,2:T(1,128)S(1)} %copy.336, s32[]{:T(128)} %get-tuple-element.424, s32[]{:T(128)} %constant.38.clone.1..sunk, s32[]{:T(128)} %constant.38.clone.1..sunk, s32[]{:T(128)} %constant.38.clone.1..sunk) | dynamic-update-slice | bytes 524292 | tf_op jit(solution)/shard_map/while/body/jit(dynamic_update_index_in_dim)/dynamic_update_slice | solution.py:202
  85.8 8.2 %dynamic_update_slice.19 = f32[8,128,2,256]{1,0,3,2:T(8,128)} dynamic-update-slice(f32[8,128,2,256]{1,0,3,2:T(8,128)} %get-tuple-element.428, f32[1,128,2,256]{1,0,3,2:T(1,128)S(1)} %copy.336, s32[]{:T(128)} %get-tuple-element.424, s32[]{:T(128)} %constant.38.clone.1..sunk, s32[]{:T(128)} %constant.38.clone.1..sunk, s32[]{:T(128)} %constant.38.clone.1..sunk) | dynamic-update-slice | bytes 524292 | tf_op jit(solution)/shard_map/while/body/jit(dynamic_update_index_in_dim)/dynamic_update_slice | solution.py:202
  98.6 8.2 %dynamic_update_slice.19 = f32[8,128,2,256]{1,0,3,2:T(8,128)} dynamic-update-slice(f32[8,128,2,256]{1,0,3,2:T(8,128)} %get-tuple-element.428, f32[1,128,2,256]{1,0,3,2:T(1,128)S(1)} %copy.336, s32[]{:T(128)} %get-tuple-element.424, s32[]{:T(128)} %constant.38.clone.1..sunk, s32[]{:T(128)} %constant.38.clone.1..sunk, s32[]{:T(128)} %constant.38.clone.1..sunk) | dynamic-update-slice | bytes 524292 | tf_op jit(solution)/shard_map/while/body/jit(dynamic_update_index_in_dim)/dynamic_update_slice | solution.py:202
  111.4 8.2 %dynamic_update_slice.19 = f32[8,128,2,256]{1,0,3,2:T(8,128)} dynamic-update-slice(f32[8,128,2,256]{1,0,3,2:T(8,128)} %get-tuple-element.428, f32[1,128,2,256]{1,0,3,2:T(1,128)S(1)} %copy.336, s32[]{:T(128)} %get-tuple-element.424, s32[]{:T(128)} %constant.38.clone.1..sunk, s32[]{:T(128)} %constant.38.clone.1..sunk, s32[]{:T(128)} %constant.38.clone.1..sunk) | dynamic-update-slice | bytes 524292 | tf_op jit(solution)/shard_map/while/body/jit(dynamic_update_index_in_dim)/dynamic_update_slice | solution.py:202
  124.2 8.2 %dynamic_update_slice.19 = f32[8,128,2,256]{1,0,3,2:T(8,128)} dynamic-update-slice(f32[8,128,2,256]{1,0,3,2:T(8,128)} %get-tuple-element.428, f32[1,128,2,256]{1,0,3,2:T(1,128)S(1)} %copy.336, s32[]{:T(128)} %get-tuple-element.424, s32[]{:T(128)} %constant.38.clone.1..sunk, s32[]{:T(128)} %constant.38.clone.1..sunk, s32[]{:T(128)} %constant.38.clone.1..sunk) | dynamic-update-slice | bytes 524292 | tf_op jit(solution)/shard_map/while/body/jit(dynamic_update_index_in_dim)/dynamic_update_slice | solution.py:202
  136.9 8.2 %dynamic_update_slice.19 = f32[8,128,2,256]{1,0,3,2:T(8,128)} dynamic-update-slice(f32[8,128,2,256]{1,0,3,2:T(8,128)} %get-tuple-element.428, f32[1,128,2,256]{1,0,3,2:T(1,128)S(1)} %copy.336, s32[]{:T(128)} %get-tuple-element.424, s32[]{:T(128)} %constant.38.clone.1..sunk, s32[]{:T(128)} %constant.38.clone.1..sunk, s32[]{:T(128)} %constant.38.clone.1..sunk) | dynamic-update-slice | bytes 524292 | tf_op jit(solution)/shard_map/while/body/jit(dynamic_update_index_in_dim)/dynamic_update_slice | solution.py:202
  149.7 8.2 %dynamic_update_slice.19 = f32[8,128,2,256]{1,0,3,2:T(8,128)} dynamic-update-slice(f32[8,128,2,256]{1,0,3,2:T(8,128)} %get-tuple-element.428, f32[1,128,2,256]{1,0,3,2:T(1,128)S(1)} %copy.336, s32[]{:T(128)} %get-tuple-element.424, s32[]{:T(128)} %constant.38.clone.1..sunk, s32[]{:T(128)} %constant.38.clone.1..sunk, s32[]{:T(128)} %constant.38.clone.1..sunk) | dynamic-update-slice | bytes 524292 | tf_op jit(solution)/shard_map/while/body/jit(dynamic_update_index_in_dim)/dynamic_update_slice | solution.py:202
  162.6 8.2 %dynamic_update_slice.19 = f32[8,128,2,256]{1,0,3,2:T(8,128)} dynamic-update-slice(f32[8,128,2,256]{1,0,3,2:T(8,128)} %get-tuple-element.428, f32[1,128,2,256]{1,0,3,2:T(1,128)S(1)} %copy.336, s32[]{:T(128)} %get-tuple-element.424, s32[]{:T(128)} %constant.38.clone.1..sunk, s32[]{:T(128)} %constant.38.clone.1..sunk, s32[]{:T(128)} %constant.38.clone.1..sunk) | dynamic-update-slice | bytes 524292 | tf_op jit(solution)/shard_map/while/body/jit(dynamic_update_index_in_dim)/dynamic_update_slice | solution.py:202
  172.5 2.9 all-gather.5
  177.3 12.4 %all-gather.6 = bf16[4,516,128]{2,1,0:T(8,128)(2,1)S(1)} all-gather(bf16[1,516,128]{2,1,0:T(8,128)(2,1)S(1)} %maximum_bitcast_fusion.1), channel_id=3, replica_groups=mesh['sp_0'=4,'sp_1'=4,'sp_2'=2,'tp'=4] {'sp_1'}, dimensions={0}, use_global_device_ids=true | all-gather | bytes 660480 | tf_op jit(solution)/shard_map/all_gather | solution.py:28
  191.1 11.0 %all-gather.7 = bf16[4,516,128]{2,1,0:T(8,128)(2,1)S(1)} all-gather(bf16[1,516,128]{2,1,0:T(8,128)(2,1)S(1)} %maximum_bitcast_fusion.2), channel_id=4, replica_groups=mesh['sp_0'=4,'sp_1'=4,'sp_2'=2,'tp'=4] {'sp_0'}, dimensions={0}, use_global_device_ids=true | all-gather | bytes 660480 | tf_op jit(solution)/shard_map/all_gather | solution.py:28
  202.5 1.7 reshape.1643
  205.3 1.3 fusion.47
  206.8 1.3 multiply_reduce_fusion
  208.4 1.9 copy.197
  210.2 2.5 multiply_convert_fusion
  212.8 14.4 %all_to_all.24 = bf16[4,256,512]{2,1,0:T(8,128)(2,1)S(1)} all-to-all(bf16[4,256,512]{2,1,0:T(8,128)(2,1)S(1)} %bitcast.614), channel_id=1, replica_groups=mesh['sp_0'=4,'sp_1'=4,'sp_2'=2,'tp'=4] {'tp'}, dimensions={0} | all-to-all | bytes 2097152 | tf_op jit(solution)/shard_map/all_to_all | solution.py:249
  227.7 5.9 %fusion.40 = bf16[256,2048]{1,0:T(8,128)(2,1)S(1)} fusion(bf16[256,2048]{0,1:T(8,128)(2,1)S(1)} %bitcast.607, bf16[2048,2048]{1,0:T(8,128)(2,1)} %all-gather.13.cloned.1.call-done, bf16[256,2048]{1,0:T(8,128)(2,1)S(1)} %copy-done.2), kind=kOutput, calls=%fused_computation.77 | convolution fusion | flops 2149056512 | bytes 11534336 | tf_op jit(solution)/shard_map/dot_general | solution.py:250
  234.7 44.8 %all_to_all.25 = bf16[4,256,2048]{2,1,0:T(8,128)(2,1)S(1)} all-to-all(bf16[4,256,2048]{2,1,0:T(8,128)(2,1)S(1)} %stack.2), channel_id=1, replica_groups=mesh['sp_0'=4,'sp_1'=4,'sp_2'=2,'tp'=4] {'tp'}, dimensions={0} | all-to-all | bytes 8388608 | tf_op jit(solution)/shard_map/all_to_all | solution.py:260
  279.6 2.1 copy-done
  281.7 10.1 %collective-permute-start = (bf16[2,2048]{1,0:T(2,128)(2,1)S(1)}, bf16[2,2048]{1,0:T(2,128)(2,1)S(1)}, u32[]{:S(2)}, u32[]{:S(2)}) collective-permute-start(bf16[2,2048]{1,0:T(2,128)(2,1)S(1)} %slice.352), channel_id=1, source_target_pairs={{0,4},{4,8},{8,12},{12,16},{16,20},{20,24},{24,28},{28,32},{32,36}... | collective-permute-start | bytes 24584 | tf_op jit(solution)/shard_map/ppermute | solution.py:64
  291.9 7.0 %copy.200 = bf16[16,2,1408,64]{2,3,1,0:T(8,128)(2,1)} copy(bf16[16,2,1408,64]{2,0,1,3:T(8,128)(2,1)} %bitcast.608) | data formatting | bytes 11534336 | tf_op jit(solution)/shard_map/transpose | solution.py:88
  298.9 11.9 %fusion.37 = f32[1026,1408]{1,0:T(8,128)} fusion(bf16[2048,2816]{1,0:T(8,128)(2,1)} %all-gather.15.cloned.1.call-done, bf16[1024,2048]{1,0:T(8,128)(2,1)} %bitcast.611, bf16[2,2048]{1,0:T(2,128)(2,1)S(1)} %collective-permute-done), kind=kOutput, calls=%fused_computation.69 | convolution fusion | flops 5925519360 | bytes 15748096 | tf_op jit(solution)/shard_map/dot_general | solution.py:265
  310.9 8.7 %fusion.33 = f32[1026,1408]{1,0:T(8,128)} fusion(bf16[2048,2816]{1,0:T(8,128)(2,1)S(1)} %copy-done.16, bf16[1024,2048]{1,0:T(8,128)(2,1)S(1)} %bitcast.612, bf16[2,2048]{1,0:T(2,128)(2,1)S(1)} %collective-permute-done), kind=kOutput, calls=%fused_computation.62 | convolution fusion | flops 5925519360 | bytes 15748096 | tf_op jit(solution)/shard_map/dot_general | solution.py:266
  319.6 22.6 %convolution_convert_fusion = bf16[1024,2048]{1,0:T(8,128)(2,1)} fusion(bf16[1408,2048]{0,1:T(8,128)(2,1)} %bitcast.609, f32[1026,1408]{1,0:T(8,128)} %fusion.33, f32[1026,1408]{1,0:T(8,128)} %fusion.37, f32[1408]{0:T(1024)S(1)} %get-tuple-element.181, f32[1408]{0:T(1024)S(1)} %get-tuple-element.182, f32[1408]{0:T(1024)S(1)} %get-tuple-element.180, ...), kind=kOutput, calls=%fused_computation.72 | convolution fusion | flops 5930745856 | bytes 44598272 | tf_op jit(solution)/shard_map/dot_general | solution.py:280
  342.2 45.0 %reduce-scatter.2.cloned.1.call-done = bf16[256,2048]{1,0:T(8,128)(2,1)} async-done(((bf16[1024,2048]{1,0:T(8,128)(2,1)}), bf16[256,2048]{1,0:T(8,128)(2,1)}) %reduce-scatter.2.cloned.1.call-update) | async-done | bytes 1048592 | tf_op jit(solution)/shard_map/reduce_scatter | solution.py:279
  387.2 2.6 fusion.44
  (362 shorter events, 47.8 us)
Async XLA Ops:
  6.5 52.6 %all-gather.17.cloned.1.call-start = ((), (), s32[]{:S(2)}) async-start(), calls=%async_computation.6 | async-start | bytes 3063808 | tf_op jit(solution)/shard_map/all_gather | solution.py:85
  7.3 220.4 %all-gather.13.cloned.1.call-start = ((), (), s32[]{:S(2)}) async-start(), calls=%async_computation.3 | async-start | bytes 10485760 | tf_op jit(solution)/shard_map/all_gather | solution.py:248
  8.0 283.9 %all-gather.19.cloned.1.call-start = ((), (), s32[]{:S(2)}) async-start(), calls=%async_computation.7 | async-start | bytes 8650752 | tf_op jit(solution)/shard_map/all_gather | solution.py:85
  59.1 3.9 copy-start.7
  59.2 3.9 copy-start.8
  59.2 4.9 %copy-start.12 = (f32[1024,2]{0,1:T(2,128)S(1)}, f32[1024,2]{0,1:T(2,128)}, u32[]{:S(2)}) copy-start(f32[1024,2]{0,1:T(2,128)} %param.25) | copy-start | bytes 24580
  59.2 4.9 %copy-start.13 = (f32[1024,2]{0,1:T(2,128)S(1)}, f32[1024,2]{0,1:T(2,128)}, u32[]{:S(2)}) copy-start(f32[1024,2]{0,1:T(2,128)} %param.24) | copy-start | bytes 24580
  63.0 2.7 copy-start.14
  63.0 2.9 copy-start.3
  63.0 235.9 %all-gather.15.cloned.1.call-start = ((), (), s32[]{:S(2)}) async-start(), calls=%async_computation.4 | async-start | bytes 11894784 | tf_op jit(solution)/shard_map/all_gather | solution.py:69
  63.9 323.3 %reduce-scatter.2.cloned.1.call-start = ((), (), s32[]{:S(2)}) async-start(), calls=%async_computation.5 | async-start | bytes 5242880 | tf_op jit(solution)/shard_map/reduce_scatter | solution.py:279
  171.1 31.0 %copy-start.6 = (f32[8,128,2]{2,1,0:T(8,128)S(1)}, f32[8,128,2]{2,1,0:T(8,128)}, u32[]{:S(2)}) copy-start(f32[8,128,2]{2,1,0:T(8,128)} %get-tuple-element.72) | copy-start | bytes 24580
  171.1 31.2 %copy-start.5 = (f32[8,128,2]{2,1,0:T(8,128)S(1)}, f32[8,128,2]{2,1,0:T(8,128)}, u32[]{:S(2)}) copy-start(f32[8,128,2]{2,1,0:T(8,128)} %get-tuple-element.77) | copy-start | bytes 24580
  204.3 2.6 copy-start.4
  206.8 1.3 copy-start.15
  210.2 17.4 %copy-start.2 = (bf16[256,2048]{1,0:T(8,128)(2,1)S(1)}, bf16[256,2048]{1,0:T(8,128)(2,1)}, u32[]{:S(2)}) copy-start(bf16[256,2048]{1,0:T(8,128)(2,1)} %param.18) | copy-start | bytes 3145732
  227.7 6.2 %copy-start.11 = (f32[2048]{0:T(1024)S(1)}, f32[2048]{0:T(1024)}, u32[]{:S(2)}) copy-start(f32[2048]{0:T(1024)} %param.28) | copy-start | bytes 24580
  234.7 57.0 %copy-start.9 = (f32[3,1408]{1,0:T(4,128)S(1)}, f32[3,1408]{1,0:T(4,128)}, u32[]{:S(2)}) copy-start(f32[3,1408]{1,0:T(4,128)} %param.32) | copy-start | bytes 50692
  234.7 57.0 %copy-start.10 = (f32[3,1408]{1,0:T(4,128)S(1)}, f32[3,1408]{1,0:T(4,128)}, u32[]{:S(2)}) copy-start(f32[3,1408]{1,0:T(4,128)} %param.31) | copy-start | bytes 50692
  279.6 2.1 copy-start
  281.7 17.3 %collective-permute-start = (bf16[2,2048]{1,0:T(2,128)(2,1)S(1)}, bf16[2,2048]{1,0:T(2,128)(2,1)S(1)}, u32[]{:S(2)}, u32[]{:S(2)}) collective-permute-start(bf16[2,2048]{1,0:T(2,128)(2,1)S(1)} %slice.352), channel_id=1, source_target_pairs={{0,4},{4,8},{8,12},{12,16},{16,20},{20,24},{24,28},{28,32},{32,36}... | collective-permute-start | bytes 24584 | tf_op jit(solution)/shard_map/ppermute | solution.py:64
  298.9 12.0 %copy-start.1 = (bf16[4,256,2048]{2,1,0:T(8,128)(2,1)S(1)}, bf16[4,256,2048]{2,1,0:T(8,128)(2,1)}, u32[]{:S(2)}) copy-start(bf16[4,256,2048]{2,1,0:T(8,128)(2,1)} %copy-done) | copy-start | bytes 12582916
  298.9 12.0 %copy-start.16 = (bf16[2048,2816]{1,0:T(8,128)(2,1)S(1)}, bf16[2048,2816]{1,0:T(8,128)(2,1)}, u32[]{:S(2)}) copy-start(bf16[2048,2816]{1,0:T(8,128)(2,1)} %all-gather.15.cloned.1.call-done) | copy-start | bytes 34603012
Sparse Core Ops, SparseCore 0:
  9.5 49.5 all-gather.16
  60.8 82.5 all-gather.12
  145.1 20.1 all-gather.18
  167.4 63.4 all-gather.14
  342.4 44.8 reduce-scatter.1
